TPU v7x, 32 devices: a whole 2x2x4 slice. The times are simulated.
32 devices in a mesh: sp: 8 (over z, y), tp: 4 (over x, core).
Axes of the slice: x: 2, y: 2, z: 4, core: 2. Of those that a mesh axis runs over, the one named last changes fastest.
Arguments:
- residual: bfloat16 [8192, 2048], P(('sp', 'tp')), may hold values from -6 to 6
- pool_input: bfloat16 [8192, 1024], P('sp', 'tp'), may hold values from -6 to 6
- doc_ids: int32 [8192], P('sp'), may hold values from 0 to 3, never falling along the last dimension, each value on 1 to 4096 neighbouring positions
- pool_map: bfloat16 [4, 256, 256], P('tp'), may hold values from -0.375 to 0.375
- pool_scale: float32 [1024], P('tp'), may hold values from 0.1 to 1.9
- out_weight: bfloat16 [1024, 2048], replicated, may hold values from -0.1875 to 0.1875
- mix_gain: float32 [2048], replicated, may hold values from 0.1 to 1.9
- mix_shift: float32 [2048], replicated, may hold values from -1.75 to 1.75
- group_router: bfloat16 [2048, 4], replicated, may hold values from -0.125 to 0.125
- expert_router: bfloat16 [2048, 8], replicated, may hold values from -0.125 to 0.125
- expert_gate: bfloat16 [8, 2048, 512], P('sp'), may hold values from -0.375 to 0.375
- expert_up: bfloat16 [8, 2048, 512], P('sp'), may hold values from -0.375 to 0.375
- expert_down: bfloat16 [8, 512, 2048], P('sp'), may hold values from -0.75 to 0.75
- routes: int32 [8192, 2], P(('sp', 'tp')), may hold values from 0 to 7, as said below
- ffn_gain: float32 [2048], replicated, may hold values from 0.1 to 1.9
- ffn_shift: float32 [2048], replicated, may hold values from -1.75 to 1.75
Outputs:
- layer_out: bfloat16 [8192, 2048], P(('sp', 'tp'))
Inputs may be any that keep to these rules, and one draw needn't show every extreme that they name: `doc_ids`: document numbers never fall along the positions; each document has 1 to 4096 positions. `routes`: A token names 2 different experts. In each aligned block of half of one device's 256 rows, 4 experts are named exactly 64 times each and the others not at all.
All inputs are finite; a program needn't handle non-finite values.
Results may differ from a plain program's by a relative error of at most 0.0073.
Values may be sent and summed in bfloat16 or wider, within the bound.
A program may use at most 128 MiB of HBM per device.

v0:
```python
import jax
import jax.numpy as jnp
from jax import lax
from jax.sharding import PartitionSpec as P

skip_scale = 2.0**0.5
epsilon = 1e-05


def from_behind(block, axis, distance):
    devices = range(lax.axis_size(axis))
    route = [(i - distance, i) for i in devices if i - distance in devices]
    return lax.ppermute(block, axis, route)


def layer_norm(values, norm_gain, norm_shift):
    center = values - jnp.mean(values, axis=-1, keepdims=True)
    spread = jnp.mean(center * center, axis=-1, keepdims=True)
    return center * lax.rsqrt(spread + epsilon) * norm_gain + norm_shift


def route_weights(normed, chosen, group_router, expert_router):
    group_logits = jnp.dot(normed, group_router, preferred_element_type=jnp.float32)
    expert_logits = jnp.dot(normed, expert_router, preferred_element_type=jnp.float32)
    group_count = group_logits.shape[1]
    expert_count = expert_logits.shape[1]
    group_exp = jnp.exp(group_logits)
    group_prob = group_exp / jnp.sum(group_exp, axis=1, keepdims=True)
    expert_ids = jnp.arange(expert_count, dtype=jnp.int32)
    picked = jnp.sum(
        jnp.where(chosen[:, :, None] == expert_ids[None, None, :], expert_logits[:, None, :], 0.0),
        axis=2,
    )
    picked_exp = jnp.exp(picked)
    pair_share = picked_exp / jnp.sum(picked_exp, axis=1, keepdims=True)
    group_of = chosen // (expert_count // group_count)
    group_ids = jnp.arange(group_count, dtype=jnp.int32)
    group_share = jnp.sum(
        jnp.where(group_of[:, :, None] == group_ids[None, None, :], group_prob[:, None, :], 0.0),
        axis=2,
    )
    return group_share * pair_share


def expert_ffn(arrived, expert_gate, expert_up, expert_down):
    sources, slot_count, width = arrived.shape
    gathered = arrived.reshape(sources * slot_count, width)
    gate_out = jnp.dot(gathered, expert_gate[0], preferred_element_type=jnp.float32)
    up_out = jnp.dot(gathered, expert_up[0], preferred_element_type=jnp.float32)
    hidden = (jax.nn.silu(gate_out) * up_out).astype(jnp.bfloat16)
    result = jnp.dot(hidden, expert_down[0], preferred_element_type=jnp.float32).astype(
        jnp.bfloat16
    )
    return result.reshape(sources, slot_count, width)


def fill_slots(normed, chosen, capacity, expert_count):
    flat_routes = chosen.reshape(-1)
    entry_count = flat_routes.shape[0]
    onehot = (flat_routes[:, None] == jnp.arange(expert_count, dtype=jnp.int32)[None, :]).astype(
        jnp.int32
    )
    slot_rank = jnp.sum((jnp.cumsum(onehot, axis=0) - onehot) * onehot, axis=1)
    slot_index = flat_routes * capacity + slot_rank
    token_ids = jnp.arange(entry_count, dtype=jnp.int32) // chosen.shape[1]
    source_row = (
        jnp.full((expert_count * capacity,), normed.shape[0], jnp.int32)
        .at[slot_index]
        .set(token_ids)
    )
    padded = jnp.concatenate([normed, jnp.zeros((1, normed.shape[1]), normed.dtype)], axis=0)
    outgoing = jnp.take(padded, source_row, axis=0).reshape(expert_count, capacity, normed.shape[1])
    return (outgoing, slot_index)


def combine_rows(returned, slot_index, weight):
    flat_out = returned.reshape(-1, returned.shape[2])
    picked = jnp.take(flat_out, slot_index, axis=0).reshape(
        weight.shape[0], weight.shape[1], flat_out.shape[1]
    )
    return jnp.sum(weight[:, :, None] * picked.astype(jnp.float32), axis=1)


def on_device(
    residual,
    pool_input,
    doc_ids,
    pool_map,
    pool_scale,
    out_weight,
    mix_gain,
    mix_shift,
    group_router,
    expert_router,
    expert_gate,
    expert_up,
    expert_down,
    routes,
    ffn_gain,
    ffn_shift,
):
    seq_rows = pool_input.shape[0]
    reach_rows = 15
    expert_count = lax.axis_size("sp")
    tp_count = lax.axis_size("tp")
    window = jnp.left_shift(jnp.int32(2), lax.axis_index("tp"))
    first_row = lax.axis_index("sp") * seq_rows
    tail_values, tail_docs = from_behind(
        (pool_input[seq_rows - reach_rows :], doc_ids[seq_rows - reach_rows :]), "sp", 1
    )
    source = jnp.concatenate([tail_values, pool_input], axis=0).astype(jnp.float32)
    all_docs = jnp.concatenate([tail_docs, doc_ids], axis=0)
    positions = first_row - reach_rows + jnp.arange(seq_rows + reach_rows, dtype=jnp.int32)
    running = jnp.zeros((seq_rows, source.shape[1]), jnp.float32)
    weight_sum = jnp.zeros((seq_rows, 1), jnp.float32)
    for offset in range(reach_rows + 1):
        begin_row = reach_rows - offset
        earlier = source[begin_row : begin_row + seq_rows]
        keep_mask = (
            (all_docs[begin_row : begin_row + seq_rows] == doc_ids)
            & (positions[begin_row : begin_row + seq_rows] >= 0)
            & (offset < window)
        )
        same_doc = keep_mask.astype(jnp.float32)[:, None]
        running = running + same_doc * earlier
        weight_sum = weight_sum + same_doc
    pooled = (running / weight_sum - source[reach_rows:]).astype(jnp.bfloat16)
    mixed = (jnp.dot(pooled, pool_map[0], preferred_element_type=jnp.float32) * pool_scale).astype(
        jnp.bfloat16
    )
    row_count = seq_rows // tp_count
    blocks = mixed.reshape(tp_count, row_count, mixed.shape[1])
    branch = jnp.einsum(
        "abc,cd->abd",
        lax.all_to_all(blocks, "tp", split_axis=0, concat_axis=2, tiled=True),
        out_weight,
        preferred_element_type=jnp.float32,
    )[0]
    normed = layer_norm(
        skip_scale * residual.astype(jnp.float32) + branch, mix_gain, mix_shift
    ).astype(jnp.bfloat16)
    weight = route_weights(normed, routes, group_router, expert_router)
    half_most = row_count * routes.shape[1] // expert_count
    half_rows = row_count // 2
    routed_parts = []
    for piece_index in range(2):
        rows_here = slice(piece_index * half_rows, (piece_index + 1) * half_rows)
        outgoing, slot_index = fill_slots(
            normed[rows_here], routes[rows_here], half_most, expert_count
        )
        returned = lax.all_to_all(
            expert_ffn(
                lax.all_to_all(outgoing, "sp", split_axis=0, concat_axis=0, tiled=True),
                expert_gate,
                expert_up,
                expert_down,
            ),
            "sp",
            split_axis=0,
            concat_axis=0,
            tiled=True,
        )
        routed_parts.append(combine_rows(returned, slot_index, weight[rows_here]))
    routed = jnp.concatenate(routed_parts, axis=0)
    return layer_norm(skip_scale * normed.astype(jnp.float32) + routed, ffn_gain, ffn_shift).astype(
        jnp.bfloat16
    )


def solution(mesh):
    in_specs = (
        P(("sp", "tp"), None),
        P("sp", "tp"),
        P("sp"),
        P("tp", None, None),
        P("tp"),
        P(),
        P(),
        P(),
        P(),
        P(),
        P("sp", None, None),
        P("sp", None, None),
        P("sp", None, None),
        P(("sp", "tp"), None),
        P(),
        P(),
    )
    out_specs = P(("sp", "tp"), None)
    return jax.shard_map(
        on_device, mesh=mesh, in_specs=in_specs, out_specs=out_specs, check_vma=False
    )
```

profile of v0, /device:TPU:0, one launch (start us, length us, event | category | flops | bytes accessed | tf_op | source)
XLA Modules:
  0.0 278.6 jit_solution(920806730677547964)
XLA Ops:
  0.0 0.9 slice.180
  0.9 4.9 %collective-permute-start = (bf16[15,256]{1,0:T(8,128)(2,1)S(1)}, bf16[15,256]{1,0:T(8,128)(2,1)S(1)}, u32[]{:S(2)}, u32[]{:S(2)}) collective-permute-start(bf16[15,256]{1,0:T(8,128)(2,1)S(1)} %slice.180), channel_id=1, source_target_pairs={{0,4},{4,8},{8,12},{12,16},{16,20},{20,24},{24,28},{1,5},{5,9},{9,... | collective-permute-start | bytes 23048 | tf_op jit(solution)/shard_map/ppermute | solution.py:13
  5.8 0.8 slice.182
  6.5 3.4 %collective-permute-start.1 = (s32[15]{0:T(128)S(1)}, s32[15]{0:T(128)S(1)}, u32[]{:S(2)}, u32[]{:S(2)}) collective-permute-start(s32[15]{0:T(128)S(1)} %slice.182), channel_id=1, source_target_pairs={{0,4},{4,8},{8,12},{12,16},{16,20},{20,24},{24,28},{1,5},{5,9},{9,... | collective-permute-start | bytes 188 | tf_op jit(solution)/shard_map/ppermute | solution.py:13
  9.9 0.7 fusion.152
  10.7 0.1 copy.38
  10.8 0.1 eq.154
  10.9 0.1 eq.150
  11.1 0.1 copy.40
  11.2 0.1 mul.304
  11.4 0.6 reduce-window.16
  12.0 0.2 slice_reduce_fusion
  12.3 1.4 scatter_custom_fusion.1
  13.7 1.4 add_add_fusion
  15.2 1.2 maximum_convert_fusion
  16.4 4.5 %fusion.16 = bf16[1024,256]{1,0:T(8,128)(2,1)S(1)} fusion(f32[256]{0:T(256)S(1)} %copy-done.14, f32[1039,256]{1,0:T(8,128)S(1)} %maximum_convert_fusion, f32[1024]{0:T(1024)S(1)} %get-tuple-element.11, f32[1024]{0:T(1024)S(1)} %get-tuple-element.27, f32[1024]{0:T(1024)S(1)} %get-tuple-element.26, f32[1024]{0:T(1024)S(1)} %get-tuple-element.25, ...), kind=kOutput, calls=%fused_computation.31 | convolution fusion | flops 143654912 | bytes 17503232 | tf_op jit(solution)/shard_map/dot_general | solution.py:128
  20.8 1.0 copy.32
  21.8 3.5 %all-to-all-start = ((bf16[4,256,256]{1,2,0:T(8,128)(2,1)}), bf16[4,256,256]{1,2,0:T(8,128)(2,1)S(1)}, u32[]{:S(2)}, u32[]{:S(2)}) async-start(bf16[4,256,256]{1,2,0:T(8,128)(2,1)} %copy.32), calls=%async_computation | async-start | bytes 1048576 | tf_op jit(solution)/shard_map/all_to_all | solution.py:135
  25.4 8.7 %all-to-all-done = bf16[4,256,256]{1,2,0:T(8,128)(2,1)S(1)} async-done(((bf16[4,256,256]{1,2,0:T(8,128)(2,1)}), bf16[4,256,256]{1,2,0:T(8,128)(2,1)S(1)}, u32[]{:S(2)}, u32[]{:S(2)}) %all-to-all-start) | async-done | bytes 524320 | tf_op jit(solution)/shard_map/all_to_all | solution.py:135
  34.1 3.8 %fusion.153 = (f32[256]{0:T(256)S(1)}, f32[256,2048]{1,0:T(8,128)S(1)}) fusion(bf16[256,1024]{0,1:T(8,128)(2,1)S(1)} %bitcast.76, bf16[1024,2048]{1,0:T(8,128)(2,1)} %param.25, bf16[256,2048]{1,0:T(8,128)(2,1)} %param.20), kind=kOutput, calls=%fused_computation.255 | convolution fusion | flops 1075838720 | bytes 7865344 | tf_op jit(solution)/shard_map/abc,cd->abd/dot_general | solution.py:133
  38.0 0.4 multiply_reduce_fusion.3
  38.4 0.3 copy-done.5
  38.7 0.5 add_convert_fusion.1
  39.2 0.1 copy-done.1
  39.3 0.9 copy-done.3
  40.3 3.3 %gather_fusion.2 = bf16[512,2048]{1,0:T(8,128)(2,1)} fusion(bf16[129,2048]{1,0:T(8,128)(2,1)S(1)} %concatenate.18, s32[1024]{0:T(1024)S(1)} %pad_clamp_fusion.1), kind=kCustom, calls=%fused_computation.2.clone | custom fusion | bytes 4196352 | tf_op jit(solution)/shard_map/jit(_take)/gather | solution.py:72
  43.6 3.2 %broadcast_select_fusion = bf16[512,2048]{1,0:T(8,128)(2,1)} fusion(bf16[512,2048]{1,0:T(8,128)(2,1)} %gather_fusion.2, pred[512]{0:T(512)(128)(4,1)S(1)} %compare_and_fusion.1), kind=kLoop, calls=%fused_computation.26 | loop fusion | flops 1048576 | bytes 4194816 | tf_op jit(solution)/shard_map/jit(_take)/select_n | solution.py:72
  46.8 5.0 %all-to-all-start.3 = ((bf16[8,64,2048]{2,1,0:T(8,128)(2,1)}), bf16[8,64,2048]{2,1,0:T(8,128)(2,1)}, u32[]{:S(2)}, u32[]{:S(2)}) async-start(bf16[8,64,2048]{2,1,0:T(8,128)(2,1)} %bitcast.74), calls=%async_computation.3 | async-start | bytes 4194304 | tf_op jit(solution)/shard_map/all_to_all | solution.py:153
  51.8 0.1 copy.34
  51.9 0.1 eq.146
  52.0 0.1 eq.142
  52.2 0.1 copy.36
  52.3 0.1 mul.296
  52.4 0.6 reduce-window.14
  53.0 0.2 slice_reduce_fusion.1
  53.4 1.4 scatter_custom_fusion
  54.9 1.2 slice_select_fusion
  56.0 3.3 %gather_fusion = bf16[512,2048]{1,0:T(8,128)(2,1)} fusion(bf16[129,2048]{1,0:T(8,128)(2,1)S(1)} %slice_select_fusion, s32[1024]{0:T(1024)S(1)} %pad_clamp_fusion.3), kind=kCustom, calls=%fused_computation.clone | custom fusion | bytes 4196352 | tf_op jit(solution)/shard_map/jit(_take)/gather | solution.py:72
  59.3 3.2 %broadcast_select_fusion.1 = bf16[512,2048]{1,0:T(8,128)(2,1)} fusion(bf16[512,2048]{1,0:T(8,128)(2,1)} %gather_fusion, pred[512]{0:T(512)(128)(4,1)S(1)} %compare_and_fusion.3), kind=kLoop, calls=%fused_computation.27 | loop fusion | flops 1048576 | bytes 4194816 | tf_op jit(solution)/shard_map/jit(_take)/select_n | solution.py:72
  62.5 37.3 %all-to-all-done.3 = bf16[8,64,2048]{2,1,0:T(8,128)(2,1)} async-done(((bf16[8,64,2048]{2,1,0:T(8,128)(2,1)}), bf16[8,64,2048]{2,1,0:T(8,128)(2,1)}, u32[]{:S(2)}, u32[]{:S(2)}) %all-to-all-start.3) | async-done | bytes 2097184 | tf_op jit(solution)/shard_map/all_to_all | solution.py:153
  99.8 4.3 %all-to-all-start.1 = ((bf16[8,64,2048]{2,1,0:T(8,128)(2,1)}), bf16[8,64,2048]{2,1,0:T(8,128)(2,1)}, u32[]{:S(2)}, u32[]{:S(2)}) async-start(bf16[8,64,2048]{2,1,0:T(8,128)(2,1)} %bitcast.75), calls=%async_computation.1 | async-start | bytes 4194304 | tf_op jit(solution)/shard_map/all_to_all | solution.py:153
  104.2 3.5 %fusion.6 = f32[512,512]{1,0:T(8,128)S(1)} fusion(bf16[512,2048]{1,0:T(8,128)(2,1)} %bitcast.21, bf16[1,2048,512]{2,1,0:T(8,128)(2,1)} %param.30), kind=kOutput, calls=%fused_computation.16 | convolution fusion | flops 1073741824 | bytes 5242880 | tf_op jit(solution)/shard_map/dot_general | solution.py:48
  107.7 6.0 %convolution_convert_fusion = bf16[512,2048]{1,0:T(8,128)(2,1)} fusion(bf16[1,512,2048]{2,1,0:T(8,128)(2,1)S(1)} %copy-done, bf16[512,2048]{1,0:T(8,128)(2,1)} %bitcast.21, bf16[1,2048,512]{2,1,0:T(8,128)(2,1)} %param.31, f32[512,512]{1,0:T(8,128)S(1)} %fusion.6), kind=kOutput, calls=%fused_computation.6 | convolution fusion | flops 2150105088 | bytes 9437184 | tf_op jit(solution)/shard_map/dot_general | solution.py:51
  113.7 38.3 %all-to-all-done.1 = bf16[8,64,2048]{2,1,0:T(8,128)(2,1)} async-done(((bf16[8,64,2048]{2,1,0:T(8,128)(2,1)}), bf16[8,64,2048]{2,1,0:T(8,128)(2,1)}, u32[]{:S(2)}, u32[]{:S(2)}) %all-to-all-start.1) | async-done | bytes 2097184 | tf_op jit(solution)/shard_map/all_to_all | solution.py:153
  152.0 4.5 %all-to-all-start.4 = ((bf16[8,64,2048]{2,1,0:T(8,128)(2,1)}), bf16[8,64,2048]{2,1,0:T(8,128)(2,1)}, u32[]{:S(2)}, u32[]{:S(2)}) async-start(bf16[8,64,2048]{2,1,0:T(8,128)(2,1)} %bitcast.78), calls=%async_computation.4 | async-start | bytes 4194304 | tf_op jit(solution)/shard_map/all_to_all | solution.py:151
  156.5 3.5 %fusion.8 = f32[512,512]{1,0:T(8,128)S(1)} fusion(bf16[512,2048]{1,0:T(8,128)(2,1)} %bitcast.10, bf16[1,2048,512]{2,1,0:T(8,128)(2,1)} %param.30), kind=kOutput, calls=%fused_computation.18 | convolution fusion | flops 1073741824 | bytes 5242880 | tf_op jit(solution)/shard_map/dot_general | solution.py:48
  160.0 6.0 %convolution_convert_fusion.1 = bf16[512,2048]{1,0:T(8,128)(2,1)} fusion(bf16[1,512,2048]{2,1,0:T(8,128)(2,1)S(1)} %copy-done, bf16[512,2048]{1,0:T(8,128)(2,1)} %bitcast.10, bf16[1,2048,512]{2,1,0:T(8,128)(2,1)} %param.31, f32[512,512]{1,0:T(8,128)S(1)} %fusion.8), kind=kOutput, calls=%fused_computation.7 | convolution fusion | flops 2150105088 | bytes 9437184 | tf_op jit(solution)/shard_map/dot_general | solution.py:51
  166.0 38.3 %all-to-all-done.4 = bf16[8,64,2048]{2,1,0:T(8,128)(2,1)} async-done(((bf16[8,64,2048]{2,1,0:T(8,128)(2,1)}), bf16[8,64,2048]{2,1,0:T(8,128)(2,1)}, u32[]{:S(2)}, u32[]{:S(2)}) %all-to-all-start.4) | async-done | bytes 2097184 | tf_op jit(solution)/shard_map/all_to_all | solution.py:151
  204.3 4.5 %all-to-all-start.2 = ((bf16[8,64,2048]{2,1,0:T(8,128)(2,1)}), bf16[8,64,2048]{2,1,0:T(8,128)(2,1)}, u32[]{:S(2)}, u32[]{:S(2)}) async-start(bf16[8,64,2048]{2,1,0:T(8,128)(2,1)} %bitcast.77), calls=%async_computation.2 | async-start | bytes 4194304 | tf_op jit(solution)/shard_map/all_to_all | solution.py:151
  208.9 0.4 fusion.155
  209.3 0.4 fusion.154
  209.8 0.1 copy.37
  209.9 0.1 copy.33
  210.0 4.2 %gather_fusion.3 = bf16[256,2048]{1,0:T(8,128)(2,1)S(1)} fusion(bf16[512,2048]{1,0:T(8,128)(2,1)} %bitcast.23, s32[1024]{0:T(1024)S(1)} %pad_clamp_fusion), kind=kCustom, calls=%fused_computation.3.clone | custom fusion | bytes 2098176 | tf_op jit(solution)/shard_map/jit(_take)/gather | solution.py:78
  214.3 1.6 select_convert_fusion
  215.9 3.5 %reshape.223 = f32[128,2,2048]{2,1,0:T(2,128)} reshape(f32[256,2048]{1,0:T(8,128)} %select_convert_fusion) | data formatting | bytes 4194304 | tf_op jit(solution)/shard_map/convert_element_type | solution.py:81
  219.4 37.1 %all-to-all-done.2 = bf16[8,64,2048]{2,1,0:T(8,128)(2,1)} async-done(((bf16[8,64,2048]{2,1,0:T(8,128)(2,1)}), bf16[8,64,2048]{2,1,0:T(8,128)(2,1)}, u32[]{:S(2)}, u32[]{:S(2)}) %all-to-all-start.2) | async-done | bytes 2097184 | tf_op jit(solution)/shard_map/all_to_all | solution.py:151
  256.5 4.2 %gather_fusion.1 = bf16[256,2048]{1,0:T(8,128)(2,1)S(1)} fusion(bf16[512,2048]{1,0:T(8,128)(2,1)} %bitcast.15, s32[1024]{0:T(1024)S(1)} %pad_clamp_fusion.2), kind=kCustom, calls=%fused_computation.1.clone | custom fusion | bytes 2098176 | tf_op jit(solution)/shard_map/jit(_take)/gather | solution.py:78
  260.7 1.6 select_convert_fusion.1
  262.3 3.5 %reshape.222 = f32[128,2,2048]{2,1,0:T(2,128)} reshape(f32[256,2048]{1,0:T(8,128)} %select_convert_fusion.1) | data formatting | bytes 4194304 | tf_op jit(solution)/shard_map/convert_element_type | solution.py:81
  265.7 8.5 %multiply_reduce_fusion.1 = (f32[128,2048]{1,0:T(8,128)S(1)}, f32[128,2048]{1,0:T(8,128)S(1)}) fusion(f32[128,2,2048]{2,1,0:T(2,128)} %reshape.223, f32[128,2]{1,0:T(8,128)S(1)} %copy.37, f32[128,2,2048]{2,1,0:T(2,128)} %reshape.222, f32[128,2]{1,0:T(8,128)S(1)} %copy.33), kind=kLoop, calls=%fused_computation.22 | loop fusion | flops 1572864 | bytes 6293504 | tf_op jit(solution)/shard_map/reduce_sum | solution.py:81
  274.3 0.7 fusion.135
  275.0 0.8 multiply_reduce_fusion
  275.8 2.8 %add_convert_fusion = bf16[256,2048]{1,0:T(8,128)(2,1)} fusion(f32[2048]{0:T(1024)S(1)} %copy-done.10, f32[2048]{0:T(1024)S(1)} %copy-done.11, f32[256]{0:T(256)S(1)} %add_rsqrt_fusion, f32[256]{0:T(256)S(1)} %broadcast_multiply_fusion.2, f32[128,2048]{1,0:T(8,128)S(1)} %get-tuple-element.38, f32[128,2048]{1,0:T(8,128)S(1)} %get-tuple-element.39, ...), kind=kLoop, calls=%fused_computation.20 | loop fusion | flops 7340032 | bytes 5279744 | tf_op jit(solution)/shard_map/convert_element_type | solution.py:165
  (64 shorter events, 0.7 us)
Async XLA Ops:
  0.0 107.6 %copy-start = (bf16[1,512,2048]{2,1,0:T(8,128)(2,1)S(1)}, bf16[1,512,2048]{2,1,0:T(8,128)(2,1)}, u32[]{:S(2)}) copy-start(bf16[1,512,2048]{2,1,0:T(8,128)(2,1)} %param.32) | copy-start | bytes 6291460
  0.0 16.3 %copy-start.14 = (f32[256]{0:T(256)S(1)}, f32[256]{0:T(256)}, u32[]{:S(2)}) copy-start(f32[256]{0:T(256)} %param.24) | copy-start | bytes 3076
  0.0 16.4 %copy-start.13 = (bf16[1,256,256]{2,1,0:T(8,128)(2,1)S(1)}, bf16[1,256,256]{2,1,0:T(8,128)(2,1)}, u32[]{:S(2)}) copy-start(bf16[1,256,256]{2,1,0:T(8,128)(2,1)} %param.23) | copy-start | bytes 393220
  0.9 14.3 %collective-permute-start = (bf16[15,256]{1,0:T(8,128)(2,1)S(1)}, bf16[15,256]{1,0:T(8,128)(2,1)S(1)}, u32[]{:S(2)}, u32[]{:S(2)}) collective-permute-start(bf16[15,256]{1,0:T(8,128)(2,1)S(1)} %slice.180), channel_id=1, source_target_pairs={{0,4},{4,8},{8,12},{12,16},{16,20},{20,24},{24,28},{1,5},{5,9},{9,... | collective-permute-start | bytes 23048 | tf_op jit(solution)/shard_map/ppermute | solution.py:13
  6.5 7.2 %collective-permute-start.1 = (s32[15]{0:T(128)S(1)}, s32[15]{0:T(128)S(1)}, u32[]{:S(2)}, u32[]{:S(2)}) collective-permute-start(s32[15]{0:T(128)S(1)} %slice.182), channel_id=1, source_target_pairs={{0,4},{4,8},{8,12},{12,16},{16,20},{20,24},{24,28},{1,5},{5,9},{9,... | collective-permute-start | bytes 188 | tf_op jit(solution)/shard_map/ppermute | solution.py:13
  21.8 12.3 %all-to-all-start = ((bf16[4,256,256]{1,2,0:T(8,128)(2,1)}), bf16[4,256,256]{1,2,0:T(8,128)(2,1)S(1)}, u32[]{:S(2)}, u32[]{:S(2)}) async-start(bf16[4,256,256]{1,2,0:T(8,128)(2,1)} %copy.32), calls=%async_computation | async-start | bytes 1048576 | tf_op jit(solution)/shard_map/all_to_all | solution.py:135
  37.9 1.4 copy-start.1
  38.0 0.7 copy-start.5
  38.0 0.8 copy-start.6
  39.3 1.0 copy-start.3
  46.8 8.0 %copy-start.12 = (pred[129]{0:T(512)(128)(4,1)S(1)}, pred[129]{0:T(512)(128)(4,1)}, u32[]{:S(2)}) copy-start(pred[129]{0:T(512)(128)(4,1)} %constant.117.clone.1) | copy-start | bytes 391
  46.8 53.0 %all-to-all-start.3 = ((bf16[8,64,2048]{2,1,0:T(8,128)(2,1)}), bf16[8,64,2048]{2,1,0:T(8,128)(2,1)}, u32[]{:S(2)}, u32[]{:S(2)}) async-start(bf16[8,64,2048]{2,1,0:T(8,128)(2,1)} %bitcast.74), calls=%async_computation.3 | async-start | bytes 4194304 | tf_op jit(solution)/shard_map/all_to_all | solution.py:153
  99.8 52.2 %all-to-all-start.1 = ((bf16[8,64,2048]{2,1,0:T(8,128)(2,1)}), bf16[8,64,2048]{2,1,0:T(8,128)(2,1)}, u32[]{:S(2)}, u32[]{:S(2)}) async-start(bf16[8,64,2048]{2,1,0:T(8,128)(2,1)} %bitcast.75), calls=%async_computation.1 | async-start | bytes 4194304 | tf_op jit(solution)/shard_map/all_to_all | solution.py:153
  152.0 52.3 %all-to-all-start.4 = ((bf16[8,64,2048]{2,1,0:T(8,128)(2,1)}), bf16[8,64,2048]{2,1,0:T(8,128)(2,1)}, u32[]{:S(2)}, u32[]{:S(2)}) async-start(bf16[8,64,2048]{2,1,0:T(8,128)(2,1)} %bitcast.78), calls=%async_computation.4 | async-start | bytes 4194304 | tf_op jit(solution)/shard_map/all_to_all | solution.py:151
  204.3 4.6 %copy-start.8 = (s32[256,2]{0,1:T(2,128)S(1)}, s32[256,2]{0,1:T(2,128)}, u32[]{:S(2)}) copy-start(s32[256,2]{0,1:T(2,128)} %param.33) | copy-start | bytes 6148
  204.3 4.6 %copy-start.4 = (bf16[256,2048]{1,0:T(8,128)(2,1)S(1)}, bf16[256,2048]{1,0:T(8,128)(2,1)}, u32[]{:S(2)}) copy-start(bf16[256,2048]{1,0:T(8,128)(2,1)} %copy-done.3) | copy-start | bytes 3145732
  204.3 4.6 %copy-start.7 = (bf16[2048,8]{0,1:T(8,128)(2,1)S(1)}, bf16[2048,8]{0,1:T(8,128)(2,1)}, u32[]{:S(2)}) copy-start(bf16[2048,8]{0,1:T(8,128)(2,1)} %param.29) | copy-start | bytes 98308
  204.3 5.1 %copy-start.9 = (bf16[2048,4]{0,1:T(4,128)(2,1)S(1)}, bf16[2048,4]{0,1:T(4,128)(2,1)}, u32[]{:S(2)}) copy-start(bf16[2048,4]{0,1:T(4,128)(2,1)} %param.28) | copy-start | bytes 49156
  204.3 52.2 %all-to-all-start.2 = ((bf16[8,64,2048]{2,1,0:T(8,128)(2,1)}), bf16[8,64,2048]{2,1,0:T(8,128)(2,1)}, u32[]{:S(2)}, u32[]{:S(2)}) async-start(bf16[8,64,2048]{2,1,0:T(8,128)(2,1)} %bitcast.77), calls=%async_computation.2 | async-start | bytes 4194304 | tf_op jit(solution)/shard_map/all_to_all | solution.py:151
  265.7 8.5 %copy-start.2 = (f32[256,2048]{1,0:T(8,128)S(1)}, f32[256,2048]{1,0:T(8,128)}, u32[]{:S(2)}) copy-start(f32[256,2048]{1,0:T(8,128)} %copy-done.1) | copy-start | bytes 6291460
  274.9 0.8 copy-start.10
  275.0 0.8 copy-start.11
where the time goes:
time: 280 us; the launch traced here: 279 us
  waiting for transfers between devices  160 us (57%)
  local copies, waits for them, and re-layouts  30.9 us (11%)
  starting transfers between devices  30.1 us (11%)
  other arithmetic  29.2 us (10%)
  matrix products  28 us (10%)
    all_to_all x2, waiting for transfers between devices, on_device(): lax.all_to_all(outgoing, 'sp', split_axis=0, concat_axis=0, tiled=True)  75.6 us
    all_to_all x2, waiting for transfers between devices, on_device(): lax.all_to_all(expert_ffn(lax.all_to_all(outgoing, 'sp', split_axis=0, co...  75.4 us
    dot_general x2, matrix products, expert_ffn(): jnp.dot(hidden, expert_down[0], preferred_element_type=jnp.float32)  12 us
    all_to_all x2, starting transfers between devices, on_device(): lax.all_to_all(outgoing, 'sp', split_axis=0, concat_axis=0, tiled=True)  9.29 us
    all_to_all x2, starting transfers between devices, on_device(): lax.all_to_all(expert_ffn(lax.all_to_all(outgoing, 'sp', split_axis=0, co...  9.03 us
    all_to_all x1, waiting for transfers between devices, on_device(): lax.all_to_all(blocks, 'tp', split_axis=0, concat_axis=2, tiled=True)  8.74 us
    reduce_sum x1, other arithmetic, combine_rows(): return jnp.sum(weight[:, :, None] * picked.astype(jnp.float32), axis=1)  8.53 us
    gather x2, local copies, waits for them, and re-layouts, combine_rows(): jnp.take(flat_out, slot_index, axis=0)  8.45 us
  transfers between devices with their start and end apart: 7, of which 5 were waited for; matrix products, arithmetic and copies ran while one was open for 16% of the time, Pallas kernels for 0%

commit v1 on v0

--- a/solution.py
+++ b/solution.py
@@ -1,6 +1,10 @@
+import functools
+
 import jax
 import jax.numpy as jnp
 from jax import lax
+from jax.experimental import pallas as pl
+from jax.experimental.pallas import tpu as pltpu
 from jax.sharding import PartitionSpec as P
 
 skip_scale = 2.0**0.5
@@ -79,6 +83,322 @@
         weight.shape[0], weight.shape[1], flat_out.shape[1]
     )
     return jnp.sum(weight[:, :, None] * picked.astype(jnp.float32), axis=1)
+
+
+MESH = pl.DeviceIdType.MESH
+group_size = 4
+
+
+def flip(index, bit):
+    return index + bit - 2 * bit * ((index // bit) % 2)
+
+
+def experts_kernel(
+    dims,
+    normed,
+    meta,
+    gate_piece,
+    up_piece,
+    own_gate,
+    own_up,
+    own_down,
+    gain,
+    shift,
+    out,
+    gate_a,
+    up_a,
+    down_a,
+    gate_b,
+    up_b,
+    down_b,
+    rows_in,
+    meta_in,
+    picked,
+    spread,
+    slot_weight,
+    hidden,
+    weighted,
+    partial,
+    passing,
+    arrived,
+    load_sems,
+    send_sems,
+    recv_sems,
+):
+    slots, expert_count = dims
+    rows, width = normed.shape
+    half = rows // 2
+    ff = own_gate.shape[2]
+    piece = gate_piece.shape[1]
+    sp, tp = lax.axis_index("sp"), lax.axis_index("tp")
+    to_y = {"sp": flip(sp, 1)}
+    to_z = {"sp": flip(sp, 2)}
+    to_far = {"sp": flip(sp, group_size)}
+    to_x = {"tp": flip(tp, 2)}
+    to_core = {"tp": flip(tp, 1)}
+
+    loads = [
+        pltpu.make_async_copy(own_gate.at[0], gate_a, load_sems.at[0]),
+        pltpu.make_async_copy(own_up.at[0], up_a, load_sems.at[1]),
+        pltpu.make_async_copy(own_down.at[0], down_a, load_sems.at[2]),
+    ]
+    for load in loads:
+        load.start()
+
+    barrier = pltpu.get_barrier_semaphore()
+    peers = (to_y, to_z, to_far, to_x, to_core)
+    for peer in peers:
+        pl.semaphore_signal(barrier, inc=1, device_id=peer, device_id_type=MESH)
+    pl.semaphore_wait(barrier, len(peers))
+
+    made = []
+
+    def send(src, dst, peer):
+        index = len(made)
+        copy = pltpu.make_async_remote_copy(
+            src_ref=src,
+            dst_ref=dst,
+            send_sem=send_sems.at[index],
+            recv_sem=recv_sems.at[index],
+            device_id=peer,
+            device_id_type=MESH,
+        )
+        copy.start()
+        made.append(copy)
+        return copy
+
+    first, second = pl.ds(0, half), pl.ds(half, half)
+
+    def cols(position):
+        return pl.ds(pl.multiple_of(position * piece, piece), piece)
+
+    mine, across, other, corner = cols(tp), cols(flip(tp, 2)), cols(flip(tp, 1)), None
+
+    meta_y = send(meta, meta_in.at[0], to_y)
+    meta_z = send(meta, meta_in.at[1], to_z)
+    rows_y1 = send(normed.at[first], rows_in.at[0, first], to_y)
+    rows_z2 = send(normed.at[second], rows_in.at[1, second], to_z)
+    down_far = send(own_down.at[0, mine], down_b.at[mine], to_far)
+    gate_x = send(gate_piece, gate_b.at[:, mine], to_x)
+    up_x = send(up_piece, up_b.at[:, mine], to_x)
+    gate_c = send(gate_piece, gate_b.at[:, mine], to_core)
+    up_c = send(up_piece, up_b.at[:, mine], to_core)
+    keep = [
+        pltpu.make_async_copy(gate_piece, gate_b.at[:, mine], load_sems.at[3]),
+        pltpu.make_async_copy(up_piece, up_b.at[:, mine], load_sems.at[4]),
+    ]
+    for load in keep:
+        load.start()
+    rows_y2 = send(normed.at[second], rows_in.at[0, second], to_y)
+    rows_z1 = send(normed.at[first], rows_in.at[1, first], to_z)
+
+    slot_ids = lax.broadcasted_iota(jnp.int32, (slots, rows), 0).astype(jnp.float32)
+    experts = (sp, flip(sp, group_size))
+
+    def select(position, row_ref, meta_ref):
+        parts = []
+        for which in range(2):
+            slot_row = meta_ref[pl.ds(experts[which], 1), :]
+            weight_row = meta_ref[pl.ds(expert_count + experts[which], 1), :]
+            match = jnp.where(slot_ids == slot_row, 1.0, 0.0)
+            slot_weight[position, pl.ds(which * slots, slots), :] = jnp.sum(
+                match * weight_row, axis=1, keepdims=True
+            )
+            parts.append(match)
+        match = jnp.concatenate(parts, axis=0)
+        spread[position] = jnp.transpose(match).astype(jnp.bfloat16)
+        match = match.astype(jnp.bfloat16)
+
+        @pl.loop(0, 4)
+        def _(step):
+            wide = width // 4
+            block = pl.ds(pl.multiple_of(step * wide, wide), wide)
+            picked[position, :, block] = jnp.dot(
+                match, row_ref[:, block], preferred_element_type=jnp.float32
+            ).astype(jnp.bfloat16)
+
+    def ffn(position, which, gate, up, down):
+        where = pl.ds(which * slots, slots)
+
+        @pl.loop(0, 2)
+        def _(step):
+            wide = ff // 2
+            block = pl.ds(pl.multiple_of(step * wide, wide), wide)
+            values = picked[position, where, :]
+            gate_out = jnp.dot(values, gate[:, block], preferred_element_type=jnp.float32)
+            up_out = jnp.dot(values, up[:, block], preferred_element_type=jnp.float32)
+            hidden[:, block] = (gate_out / (1.0 + jnp.exp(-gate_out)) * up_out).astype(
+                jnp.bfloat16
+            )
+
+        @pl.loop(0, 4)
+        def _(step):
+            wide = width // 4
+            block = pl.ds(pl.multiple_of(step * wide, wide), wide)
+            result = jnp.dot(hidden[...], down[:, block], preferred_element_type=jnp.float32)
+            weighted[position, where, block] = (
+                result * slot_weight[position, where, :]
+            ).astype(jnp.bfloat16)
+
+    def gather_back(position):
+        @pl.loop(0, 4)
+        def _(step):
+            wide = width // 4
+            block = pl.ds(pl.multiple_of(step * wide, wide), wide)
+            partial[position, :, block] = jnp.dot(
+                spread[position], weighted[position, :, block], preferred_element_type=jnp.float32
+            ).astype(jnp.bfloat16)
+
+    own, from_y, from_z, from_corner = 3, 0, 1, 2
+    select(own, normed, meta)
+    for load in loads:
+        load.wait()
+    ffn(own, 0, gate_a, up_a, down_a)
+
+    meta_y.wait_recv()
+    meta_corner = send(meta_in.at[0], meta_in.at[2], to_z)
+    rows_y1.wait_recv()
+    rows_corner1 = send(rows_in.at[0, first], rows_in.at[2, first], to_z)
+    rows_z2.wait_recv()
+    rows_corner2 = send(rows_in.at[1, second], rows_in.at[2, second], to_y)
+    gate_x.wait_recv()
+    gate_relay = send(gate_b.at[:, across], gate_b.at[:, across], to_core)
+    up_x.wait_recv()
+    up_relay = send(up_b.at[:, across], up_b.at[:, across], to_core)
+    down_far.wait_recv()
+    down_x = send(down_b.at[mine], down_b.at[mine], to_x)
+    down_c = send(down_b.at[mine], down_b.at[mine], to_core)
+
+    rows_y2.wait_recv()
+    select(from_y, rows_in.at[0], meta_in.at[0])
+    ffn(from_y, 0, gate_a, up_a, down_a)
+    meta_z.wait_recv()
+    rows_z1.wait_recv()
+    select(from_z, rows_in.at[1], meta_in.at[1])
+    ffn(from_z, 0, gate_a, up_a, down_a)
+    down_x.wait_recv()
+    down_relay = send(down_b.at[across], down_b.at[across], to_core)
+    meta_corner.wait_recv()
+    rows_corner1.wait_recv()
+    rows_corner2.wait_recv()
+    select(from_corner, rows_in.at[2], meta_in.at[2])
+    ffn(from_corner, 0, gate_a, up_a, down_a)
+    for load in keep:
+        load.wait()
+    for copy in (gate_c, up_c, gate_relay, up_relay, down_c, down_relay):
+        copy.wait_recv()
+
+    ffn(from_corner, 1, gate_b, up_b, down_b)
+    gather_back(from_corner)
+    pass_y = send(partial.at[from_corner, first], passing.at[0], to_y)
+    pass_z = send(partial.at[from_corner, second], passing.at[1], to_z)
+    ffn(from_y, 1, gate_b, up_b, down_b)
+    gather_back(from_y)
+    back_y1 = send(partial.at[from_y, first], arrived.at[0, first], to_y)
+    ffn(from_z, 1, gate_b, up_b, down_b)
+    gather_back(from_z)
+    back_z2 = send(partial.at[from_z, second], arrived.at[1, second], to_z)
+
+    def add_passing(position, where, slot):
+        partial[position, where, :] = (
+            partial[position, where, :].astype(jnp.float32) + passing[slot].astype(jnp.float32)
+        ).astype(jnp.bfloat16)
+
+    pass_y.wait_recv()
+    add_passing(from_z, first, 0)
+    back_z1 = send(partial.at[from_z, first], arrived.at[1, first], to_z)
+    pass_z.wait_recv()
+    add_passing(from_y, second, 1)
+    back_y2 = send(partial.at[from_y, second], arrived.at[0, second], to_y)
+    ffn(own, 1, gate_b, up_b, down_b)
+    for copy in (back_y1, back_z2, back_z1, back_y2):
+        copy.wait_recv()
+
+    @pl.loop(0, rows // 64)
+    def _(step):
+        block = pl.ds(pl.multiple_of(step * 64, 64), 64)
+        routed = jnp.dot(spread[own, block, :], weighted[own], preferred_element_type=jnp.float32)
+        routed = routed + arrived[0, block, :].astype(jnp.float32)
+        routed = routed + arrived[1, block, :].astype(jnp.float32)
+        values = skip_scale * normed[block, :].astype(jnp.float32) + routed
+        out[block, :] = layer_norm(values, gain[...], shift[...]).astype(jnp.bfloat16)
+
+    for copy in made:
+        copy.wait_send()
+
+
+def routing_table(chosen, weight, expert_count, capacity):
+    rows = chosen.shape[0]
+    half = rows // 2
+    onehot = (
+        chosen[:, :, None] == jnp.arange(expert_count, dtype=jnp.int32)[None, None, :]
+    ).astype(jnp.float32)
+    named = jnp.sum(onehot, axis=1)
+    before = jnp.tril(jnp.ones((half, half), jnp.bfloat16), -1)
+    rank = jnp.einsum(
+        "ab,hbe->hae",
+        before,
+        named.reshape(2, half, expert_count).astype(jnp.bfloat16),
+        preferred_element_type=jnp.float32,
+    )
+    rank = rank + jnp.arange(2, dtype=jnp.float32)[:, None, None] * capacity
+    slot = jnp.where(named > 0, rank.reshape(rows, expert_count), -1.0)
+    share = jnp.sum(onehot * weight[:, :, None], axis=1)
+    return jnp.concatenate([slot, share], axis=1).T
+
+
+def near_experts(
+    normed, weight, routes, pieces, expert_gate, expert_up, expert_down, ffn_gain, ffn_shift
+):
+    expert_count = lax.axis_size("sp")
+    rows, width = normed.shape
+    ff = expert_gate.shape[2]
+    capacity = rows // 2 * routes.shape[1] * 2 // expert_count
+    slots = 2 * capacity
+    meta = routing_table(routes, weight, expert_count, capacity)
+    vmem = pl.BlockSpec(memory_space=pltpu.VMEM)
+    anywhere = pl.BlockSpec(memory_space=pl.ANY)
+    bf16 = jnp.bfloat16
+    return pl.pallas_call(
+        functools.partial(experts_kernel, (slots, expert_count)),
+        out_shape=jax.ShapeDtypeStruct((rows, width), bf16),
+        in_specs=[vmem, vmem] + [anywhere] * 5 + [vmem, vmem],
+        out_specs=vmem,
+        scratch_shapes=[
+            pltpu.VMEM((width, ff), bf16),
+            pltpu.VMEM((width, ff), bf16),
+            pltpu.VMEM((ff, width), bf16),
+            pltpu.VMEM((width, ff), bf16),
+            pltpu.VMEM((width, ff), bf16),
+            pltpu.VMEM((ff, width), bf16),
+            pltpu.VMEM((3, rows, width), bf16),
+            pltpu.VMEM((3,) + meta.shape, jnp.float32),
+            pltpu.VMEM((4, 2 * slots, width), bf16),
+            pltpu.VMEM((4, rows, 2 * slots), bf16),
+            pltpu.VMEM((4, 2 * slots, 1), jnp.float32),
+            pltpu.VMEM((slots, ff), bf16),
+            pltpu.VMEM((4, 2 * slots, width), bf16),
+            pltpu.VMEM((3, rows, width), bf16),
+            pltpu.VMEM((2, rows // 2, width), bf16),
+            pltpu.VMEM((2, rows, width), bf16),
+            pltpu.SemaphoreType.DMA((5,)),
+            pltpu.SemaphoreType.DMA((25,)),
+            pltpu.SemaphoreType.DMA((25,)),
+        ],
+        compiler_params=pltpu.CompilerParams(
+            collective_id=0, has_side_effects=True, vmem_limit_bytes=60 * 1024 * 1024
+        ),
+    )(
+        normed,
+        meta,
+        pieces[0],
+        pieces[1],
+        expert_gate,
+        expert_up,
+        expert_down,
+        ffn_gain[None, :],
+        ffn_shift[None, :],
+    )
 
 
 def on_device(
@@ -103,6 +423,15 @@
     reach_rows = 15
     expert_count = lax.axis_size("sp")
     tp_count = lax.axis_size("tp")
+    near = expert_count == 2 * group_size and tp_count == group_size
+    if near:
+        piece = expert_gate.shape[2] // tp_count
+        begin = lax.axis_index("tp") * piece
+        swap = [(i, (i + group_size) % expert_count) for i in range(expert_count)]
+        pieces = [
+            lax.ppermute(lax.dynamic_slice_in_dim(part[0], begin, piece, axis=1), "sp", swap)
+            for part in (expert_gate, expert_up)
+        ]
     window = jnp.left_shift(jnp.int32(2), lax.axis_index("tp"))
     first_row = lax.axis_index("sp") * seq_rows
     tail_values, tail_docs = from_behind(
@@ -140,6 +469,10 @@
         skip_scale * residual.astype(jnp.float32) + branch, mix_gain, mix_shift
     ).astype(jnp.bfloat16)
     weight = route_weights(normed, routes, group_router, expert_router)
+    if near:
+        return near_experts(
+            normed, weight, routes, pieces, expert_gate, expert_up, expert_down, ffn_gain, ffn_shift
+        )
     half_most = row_count * routes.shape[1] // expert_count
     half_rows = row_count // 2
     routed_parts = []

time: 280 us -> 156 us (0.56)
  waiting for transfers between devices: 160 us -> 27.1 us
  Pallas kernels: 0 us -> 93.1 us
  other arithmetic: 29.2 us -> 1.81 us
  local copies, waits for them, and re-layouts: 30.9 us -> 8.95 us
  matrix products: 28 us -> 8.99 us
  starting transfers between devices: 30.1 us -> 14.8 us
    all_to_all x4 -> x0, waiting for transfers between devices: 151 us -> none  [the longest x2 75.6 us: on_device(): lax.all_to_all(outgoing, 'sp', split_axis=0, concat_axis=0, tiled=True)]
    pallas_call x0 -> x1, Pallas kernels: none -> 93.1 us  [near_experts(): pl.pallas_call(functools.partial(experts_kernel, (slots, expert_count)),...]
    dot_general x4 -> x1, matrix products: 18.9 us -> 0.2 us  [routing_table(): jnp.einsum('ab,hbe->hae', before, named.reshape(2, half, expert_count).as...]
    ppermute x0 -> x2, waiting for transfers between devices: none -> 18.3 us  [on_device(): lax.ppermute(lax.dynamic_slice_in_dim(part[0], begin, piece, axis=1), 'sp...]
    all_to_all x4 -> x0, starting transfers between devices: 18.3 us -> none  [the longest x2 9.29 us: on_device(): lax.all_to_all(outgoing, 'sp', split_axis=0, concat_axis=0, tiled=True)]
    gather x4 -> x0, local copies, waits for them, and re-layouts: 15.1 us -> none  [the longest x2 8.45 us: combine_rows(): jnp.take(flat_out, slot_index, axis=0)]
    reduce_sum x5 -> x2, other arithmetic: 9.39 us -> 0.04 us  [the longest x1 0.03 us: routing_table(): named = jnp.sum(onehot, axis=1)]
    convert_element_type x2 -> x0, local copies, waits for them, and re-layouts: 6.95 us -> none  [combine_rows(): return jnp.sum(weight[:, :, None] * picked.astype(jnp.float32), axis=1)]
  transfers between devices with their start and end apart: 7 -> 5, of which waited for: 5 -> 3; matrix products, arithmetic and copies ran while one was open for 16% -> 10% of each run, Pallas kernels for 0% -> 0%
where the time goes in v1:
time: 156 us; the launch traced here: 155 us
  Pallas kernels  93.1 us (60%)
  waiting for transfers between devices  27.1 us (17%)
  starting transfers between devices  14.8 us (9%)
  matrix products  8.99 us (6%)
  local copies, waits for them, and re-layouts  8.95 us (6%)
  other arithmetic  1.81 us (1%)
    pallas_call x1, Pallas kernels, near_experts(): pl.pallas_call(functools.partial(experts_kernel, (slots, expert_count)),...  93.1 us
    ppermute x2, waiting for transfers between devices, on_device(): lax.ppermute(lax.dynamic_slice_in_dim(part[0], begin, piece, axis=1), 'sp...  18.3 us
    all_to_all x1, waiting for transfers between devices, on_device(): lax.all_to_all(blocks, 'tp', split_axis=0, concat_axis=2, tiled=True)  8.73 us
    ppermute x2, starting transfers between devices, from_behind(): return lax.ppermute(block, axis, route)  8.31 us
    dot_general x1, matrix products, on_device(): jnp.dot(pooled, pool_map[0], preferred_element_type=jnp.float32)  4.46 us
    dot_general x1, matrix products, on_device(): jnp.einsum('abc,cd->abd', lax.all_to_all(blocks, 'tp', split_axis=0, conc...  3.55 us
    unnamed x27, local copies, waits for them, and re-layouts  3.47 us
    all_to_all x1, starting transfers between devices, on_device(): lax.all_to_all(blocks, 'tp', split_axis=0, concat_axis=2, tiled=True)  3.47 us
  transfers between devices with their start and end apart: 5, of which 3 were waited for; matrix products, arithmetic and copies ran while one was open for 10% of the time, Pallas kernels for 0%

profile of v1, /device:TPU:0, one launch (start us, length us, event | category | flops | bytes accessed | tf_op | source)
XLA Modules:
  0.0 155.0 jit_solution(14191232178174492312)
XLA Ops:
  0.0 0.0 copy-start
  0.0 0.0 copy-start.11
  0.0 0.0 copy-start.3
  0.0 0.0 copy-start.12
  0.0 0.8 slice.151
  0.8 4.9 %collective-permute-start.1 = (s32[15]{0:T(128)S(1)}, s32[15]{0:T(128)S(1)}, u32[]{:S(2)}, u32[]{:S(2)}) collective-permute-start(s32[15]{0:T(128)S(1)} %slice.151), channel_id=1, source_target_pairs={{0,4},{4,8},{8,12},{12,16},{16,20},{20,24},{24,28},{1,5},{5,9},{9,... | collective-permute-start | bytes 188 | tf_op jit(solution)/shard_map/ppermute | solution.py:17
  5.7 0.7 slice.149
  6.4 3.4 %collective-permute-start = (bf16[15,256]{1,0:T(8,128)(2,1)S(1)}, bf16[15,256]{1,0:T(8,128)(2,1)S(1)}, u32[]{:S(2)}, u32[]{:S(2)}) collective-permute-start(bf16[15,256]{1,0:T(8,128)(2,1)S(1)} %slice.149), channel_id=1, source_target_pairs={{0,4},{4,8},{8,12},{12,16},{16,20},{20,24},{24,28},{1,5},{5,9},{9,... | collective-permute-start | bytes 23048 | tf_op jit(solution)/shard_map/ppermute | solution.py:17
  9.9 1.1 dynamic-slice_bitcast_fusion.1
  11.0 2.7 %collective-permute-start.2 = (bf16[2048,128]{1,0:T(8,128)(2,1)S(1)}, bf16[2048,128]{1,0:T(8,128)(2,1)S(1)}, u32[]{:S(2)}, u32[]{:S(2)}) collective-permute-start(bf16[2048,128]{1,0:T(8,128)(2,1)S(1)} %dynamic-slice_bitcast_fusion.1), channel_id=1, source_target_pairs={{0,16},{4,20},{8,24},{12,28},{16,0},{20,4},{24,8},{28,12},{1,17},{... | collective-permute-start | bytes 1572872 | tf_op jit(solution)/shard_map/ppermute | solution.py:432
  13.6 1.9 %dynamic-slice_bitcast_fusion = bf16[2048,128]{1,0:T(8,128)(2,1)} fusion(bf16[1,2048,512]{2,1,0:T(8,128)(2,1)} %own_up.1, s32[]{:T(128)S(6)} %select_n.30), kind=kLoop, calls=%fused_computation.43 | loop fusion | bytes 1048580 | tf_op jit(solution)/shard_map/dynamic_slice | solution.py:432
  15.5 0.3 collective-permute-start.3
  15.8 0.0 collective-permute-done.1
  15.8 0.0 copy-done.11
  15.8 0.1 add_add_fusion
  16.0 0.0 collective-permute-done
  16.0 0.0 copy-done.3
  16.0 0.1 maximum_convert_fusion
  16.1 0.0 copy-done
  16.1 0.0 copy-done.12
  16.1 4.5 %fusion = bf16[1024,256]{1,0:T(8,128)(2,1)S(1)} fusion(f32[256]{0:T(256)S(1)} %copy-done.12, f32[1039,256]{1,0:T(8,128)S(1)} %maximum_convert_fusion, f32[1024]{0:T(1024)S(1)} %get-tuple-element.7, f32[1024]{0:T(1024)S(1)} %get-tuple-element.23, f32[1024]{0:T(1024)S(1)} %get-tuple-element.22, f32[1024]{0:T(1024)S(1)} %get-tuple-element.21, ...), kind=kOutput, calls=%fused_computation.4 | convolution fusion | flops 143654912 | bytes 17503232 | tf_op jit(solution)/shard_map/dot_general | solution.py:457
  20.6 0.0 copy-start.7
  20.6 0.0 copy-start.2
  20.6 1.0 copy.26
  21.6 3.5 %all-to-all-start = ((bf16[4,256,256]{1,2,0:T(8,128)(2,1)}), bf16[4,256,256]{1,2,0:T(8,128)(2,1)S(1)}, u32[]{:S(2)}, u32[]{:S(2)}) async-start(bf16[4,256,256]{1,2,0:T(8,128)(2,1)} %copy.26), calls=%async_computation | async-start | bytes 1048576 | tf_op jit(solution)/shard_map/all_to_all | solution.py:464
  25.1 0.0 copy-done.7
  25.2 8.7 %all-to-all-done = bf16[4,256,256]{1,2,0:T(8,128)(2,1)S(1)} async-done(((bf16[4,256,256]{1,2,0:T(8,128)(2,1)}), bf16[4,256,256]{1,2,0:T(8,128)(2,1)S(1)}, u32[]{:S(2)}, u32[]{:S(2)}) %all-to-all-start) | async-done | bytes 524320 | tf_op jit(solution)/shard_map/all_to_all | solution.py:464
  33.9 0.0 copy-done.2
  33.9 3.5 %fusion.122 = (f32[256]{0:T(256)S(1)}, f32[256,2048]{1,0:T(8,128)S(1)}) fusion(bf16[256,1024]{0,1:T(8,128)(2,1)S(1)} %bitcast.35, bf16[1024,2048]{1,0:T(8,128)(2,1)} %param.21, bf16[256,2048]{1,0:T(8,128)(2,1)S(1)} %copy-done.2), kind=kOutput, calls=%fused_computation.196 | convolution fusion | flops 1075838720 | bytes 7865344 | tf_op jit(solution)/shard_map/abc,cd->abd/dot_general | solution.py:462
  37.4 0.0 copy-start.9
  37.4 0.0 copy-start.10
  37.5 0.4 multiply_reduce_fusion
  37.8 0.0 copy-start.6
  37.8 0.3 copy-done.9
  38.1 0.0 copy-done.10
  38.2 0.0 copy-start.8
  38.2 0.5 add_convert_fusion.normed
  38.6 0.0 copy-done.6
  38.6 0.0 copy-start.1
  38.6 0.4 fusion.124
  39.1 0.0 copy-done.8
  39.1 0.4 fusion.123
  39.6 0.2 fusion.2
  39.8 0.6 maximum_bitcast_fusion.meta
  40.4 8.2 %collective-permute-done.2.gate_piece = bf16[2048,128]{1,0:T(8,128)(2,1)S(1)} collective-permute-done((bf16[2048,128]{1,0:T(8,128)(2,1)S(1)}, bf16[2048,128]{1,0:T(8,128)(2,1)S(1)}, u32[]{:S(2)}, u32[]{:S(2)}) %collective-permute-start.2) | collective-permute-done | bytes 524320 | tf_op jit(solution)/shard_map/ppermute | solution.py:432
  48.6 0.0 copy-start.4
  48.6 10.1 %collective-permute-done.3.up_piece = bf16[2048,128]{1,0:T(8,128)(2,1)S(1)} collective-permute-done((bf16[2048,128]{1,0:T(8,128)(2,1)}, bf16[2048,128]{1,0:T(8,128)(2,1)S(1)}, u32[]{:S(2)}, u32[]{:S(2)}) %collective-permute-start.3) | collective-permute-done | bytes 524320 | tf_op jit(solution)/shard_map/ppermute | solution.py:432
  58.7 0.0 copy-start.5
  58.7 0.0 copy-done.1
  58.7 0.0 copy-done.4
  58.7 0.8 copy-done.5
  59.5 93.1 %shard_map.154 = bf16[256,2048]{1,0:T(8,128)(2,1)} custom-call(bf16[256,2048]{1,0:T(8,128)(2,1)} %copy-done.1, f32[16,256]{1,0:T(8,128)} %maximum_bitcast_fusion.meta, bf16[2048,128]{1,0:T(8,128)(2,1)} %copy-done.4, bf16[2048,128]{1,0:T(8,128)(2,1)} %copy-done.5, bf16[1,2048,512]{2,1,0:T(8,128)(2,1)} %own_gate.1, bf16[1,2048,512]{2,1,0:T(8,128)(2,1)} %own_up.1, ...), custom_call_target="tpu_custom_call" | custom-call | tf_op jit(solution)/shard_map/pallas_call | solution.py:362
  152.7 2.3 %copy.28 = bf16[256,2048]{1,0:T(8,128)(2,1)} copy(bf16[256,2048]{1,0:T(8,128)(2,1)} %shard_map.154) | data formatting | bytes 2097152
  (12 shorter events, 0.1 us)
Async XLA Ops:
  0.0 16.1 %copy-start = (bf16[1,256,256]{2,1,0:T(8,128)(2,1)S(1)}, bf16[1,256,256]{2,1,0:T(8,128)(2,1)}, u32[]{:S(2)}) copy-start(bf16[1,256,256]{2,1,0:T(8,128)(2,1)} %param.19) | copy-start | bytes 393220
  0.0 15.8 %copy-start.11 = (s32[1024]{0:T(1024)S(1)}, s32[1024]{0:T(1024)}, u32[]{:S(2)}) copy-start(s32[1024]{0:T(1024)} %param.18) | copy-start | bytes 12292
  0.0 16.0 %copy-start.3 = (bf16[1024,256]{1,0:T(8,128)(2,1)S(1)}, bf16[1024,256]{1,0:T(8,128)(2,1)}, u32[]{:S(2)}) copy-start(bf16[1024,256]{1,0:T(8,128)(2,1)} %param.17) | copy-start | bytes 1572868
  0.0 16.1 %copy-start.12 = (f32[256]{0:T(256)S(1)}, f32[256]{0:T(256)}, u32[]{:S(2)}) copy-start(f32[256]{0:T(256)} %param.20) | copy-start | bytes 3076
  0.8 15.0 %collective-permute-start.1 = (s32[15]{0:T(128)S(1)}, s32[15]{0:T(128)S(1)}, u32[]{:S(2)}, u32[]{:S(2)}) collective-permute-start(s32[15]{0:T(128)S(1)} %slice.151), channel_id=1, source_target_pairs={{0,4},{4,8},{8,12},{12,16},{16,20},{20,24},{24,28},{1,5},{5,9},{9,... | collective-permute-start | bytes 188 | tf_op jit(solution)/shard_map/ppermute | solution.py:17
  6.4 9.5 %collective-permute-start = (bf16[15,256]{1,0:T(8,128)(2,1)S(1)}, bf16[15,256]{1,0:T(8,128)(2,1)S(1)}, u32[]{:S(2)}, u32[]{:S(2)}) collective-permute-start(bf16[15,256]{1,0:T(8,128)(2,1)S(1)} %slice.149), channel_id=1, source_target_pairs={{0,4},{4,8},{8,12},{12,16},{16,20},{20,24},{24,28},{1,5},{5,9},{9,... | collective-permute-start | bytes 23048 | tf_op jit(solution)/shard_map/ppermute | solution.py:17
  11.0 37.7 %collective-permute-start.2 = (bf16[2048,128]{1,0:T(8,128)(2,1)S(1)}, bf16[2048,128]{1,0:T(8,128)(2,1)S(1)}, u32[]{:S(2)}, u32[]{:S(2)}) collective-permute-start(bf16[2048,128]{1,0:T(8,128)(2,1)S(1)} %dynamic-slice_bitcast_fusion.1), channel_id=1, source_target_pairs={{0,16},{4,20},{8,24},{12,28},{16,0},{20,4},{24,8},{28,12},{1,17},{... | collective-permute-start | bytes 1572872 | tf_op jit(solution)/shard_map/ppermute | solution.py:432
  15.5 43.3 %collective-permute-start.3 = (bf16[2048,128]{1,0:T(8,128)(2,1)}, bf16[2048,128]{1,0:T(8,128)(2,1)S(1)}, u32[]{:S(2)}, u32[]{:S(2)}) collective-permute-start(bf16[2048,128]{1,0:T(8,128)(2,1)} %dynamic-slice_bitcast_fusion), channel_id=1, source_target_pairs={{0,16},{4,20},{8,24},{12,28},{16,0},{20,4},{24,8},{28,12},{1,17},{... | collective-permute-start | bytes 1572872 | tf_op jit(solution)/shard_map/ppermute | solution.py:432
  20.6 4.5 %copy-start.7 = (s32[256,2]{0,1:T(2,128)S(1)}, s32[256,2]{0,1:T(2,128)}, u32[]{:S(2)}) copy-start(s32[256,2]{0,1:T(2,128)} %param.29) | copy-start | bytes 6148
  20.6 13.3 %copy-start.2 = (bf16[256,2048]{1,0:T(8,128)(2,1)S(1)}, bf16[256,2048]{1,0:T(8,128)(2,1)}, u32[]{:S(2)}) copy-start(bf16[256,2048]{1,0:T(8,128)(2,1)} %param.16) | copy-start | bytes 3145732
  21.6 12.3 %all-to-all-start = ((bf16[4,256,256]{1,2,0:T(8,128)(2,1)}), bf16[4,256,256]{1,2,0:T(8,128)(2,1)S(1)}, u32[]{:S(2)}, u32[]{:S(2)}) async-start(bf16[4,256,256]{1,2,0:T(8,128)(2,1)} %copy.26), calls=%async_computation | async-start | bytes 1048576 | tf_op jit(solution)/shard_map/all_to_all | solution.py:464
  37.4 0.7 copy-start.9
  37.4 0.7 copy-start.10
  37.8 0.8 copy-start.6
  38.2 0.9 copy-start.8
  38.6 20.1 %copy-start.1 = (bf16[256,2048]{1,0:T(8,128)(2,1)}, bf16[256,2048]{1,0:T(8,128)(2,1)S(1)}, u32[]{:S(2)}) copy-start(bf16[256,2048]{1,0:T(8,128)(2,1)S(1)} %add_convert_fusion.normed) | copy-start | bytes 3145732
  48.6 10.1 %copy-start.4 = (bf16[2048,128]{1,0:T(8,128)(2,1)}, bf16[2048,128]{1,0:T(8,128)(2,1)S(1)}, u32[]{:S(2)}) copy-start(bf16[2048,128]{1,0:T(8,128)(2,1)S(1)} %collective-permute-done.2.gate_piece) | copy-start | bytes 1572868
  58.7 0.8 copy-start.5

commit v2 on v1

--- a/solution.py
+++ b/solution.py
@@ -95,16 +95,30 @@
 
 def experts_kernel(
     dims,
-    normed,
-    meta,
-    gate_piece,
-    up_piece,
+    residual,
+    pool_input,
+    docs,
+    pool_map,
+    pool_scale,
+    out_weight,
+    mix_gain,
+    mix_shift,
+    routers,
+    chosen,
     own_gate,
     own_up,
     own_down,
     gain,
     shift,
     out,
+    tail,
+    tail_docs,
+    mapped,
+    mixed_in,
+    projection,
+    values_in,
+    normed,
+    meta,
     gate_a,
     up_a,
     down_a,
@@ -125,28 +139,35 @@
     send_sems,
     recv_sems,
 ):
-    slots, expert_count = dims
+    slots, expert_count, group_count, tp_count = dims
     rows, width = normed.shape
     half = rows // 2
     ff = own_gate.shape[2]
-    piece = gate_piece.shape[1]
+    piece = ff // tp_count
+    seq_rows, pool_width = pool_input.shape
+    reach = tail.shape[0]
     sp, tp = lax.axis_index("sp"), lax.axis_index("tp")
     to_y = {"sp": flip(sp, 1)}
     to_z = {"sp": flip(sp, 2)}
     to_far = {"sp": flip(sp, group_size)}
     to_x = {"tp": flip(tp, 2)}
     to_core = {"tp": flip(tp, 1)}
+    to_cross = {"tp": flip(flip(tp, 1), 2)}
+    to_next = {"sp": (sp + 1) % expert_count}
+    to_previous = {"sp": (sp + expert_count - 1) % expert_count}
 
     loads = [
         pltpu.make_async_copy(own_gate.at[0], gate_a, load_sems.at[0]),
         pltpu.make_async_copy(own_up.at[0], up_a, load_sems.at[1]),
         pltpu.make_async_copy(own_down.at[0], down_a, load_sems.at[2]),
     ]
+    load_projection = pltpu.make_async_copy(out_weight, projection, load_sems.at[3])
+    load_projection.start()
     for load in loads:
         load.start()
 
     barrier = pltpu.get_barrier_semaphore()
-    peers = (to_y, to_z, to_far, to_x, to_core)
+    peers = (to_y, to_z, to_far, to_x, to_core, to_cross, to_next, to_previous)
     for peer in peers:
         pl.semaphore_signal(barrier, inc=1, device_id=peer, device_id_type=MESH)
     pl.semaphore_wait(barrier, len(peers))
@@ -172,25 +193,109 @@
     def cols(position):
         return pl.ds(pl.multiple_of(position * piece, piece), piece)
 
-    mine, across, other, corner = cols(tp), cols(flip(tp, 2)), cols(flip(tp, 1)), None
-
+    mine, across = cols(tp), cols(flip(tp, 2))
+
+    last = pl.ds(seq_rows - reach, reach)
+    tail_copy = send(pool_input.at[last], tail, to_next)
+    docs_copy = send(docs.at[last], tail_docs, to_next)
+    gate_far = send(own_gate.at[0, :, mine], gate_b.at[:, mine], to_far)
+
+    expert_rows = lax.broadcasted_iota(jnp.int32, (2 * expert_count, rows), 0)
+    named = (expert_rows == chosen[0:1, :]) | (expert_rows == chosen[1:2, :])
+    earlier = lax.broadcasted_iota(jnp.int32, (rows, rows), 0)
+    later = lax.broadcasted_iota(jnp.int32, (rows, rows), 1)
+    ahead = (earlier < later) & ((earlier < half) == (later < half))
+    rank = jnp.dot(
+        jnp.where(named, 1.0, 0.0).astype(jnp.bfloat16),
+        jnp.where(ahead, 1.0, 0.0).astype(jnp.bfloat16),
+        preferred_element_type=jnp.float32,
+    )[:expert_count]
+    named = named[:expert_count]
+    in_second = lax.broadcasted_iota(jnp.int32, (expert_count, rows), 1) >= half
+    rank = rank + jnp.where(in_second, float(slots // 2), 0.0)
+    meta[:expert_count, :] = jnp.where(named, rank, -1.0)
+
+    tail_copy.wait_recv()
+    docs_copy.wait_recv()
+    before_docs = jnp.where(sp == 0, -1, tail_docs[...])
+    all_docs = jnp.concatenate([before_docs, docs[...]], axis=0)
+    lanes = docs.shape[1]
+    steps = reach.bit_length() - 1
+    same = [
+        (pltpu.roll(all_docs, 2**step, 0) == all_docs) & (step <= tp) for step in range(steps)
+    ]
+    count = jnp.ones(all_docs.shape, jnp.float32)
+    for step in range(steps):
+        count = count + jnp.where(same[step], pltpu.roll(count, 2**step, 0), 0.0)
+    for block in range(pool_width // lanes):
+        where = slice(block * lanes, (block + 1) * lanes)
+        source = jnp.concatenate(
+            [tail[:, where].astype(jnp.float32), pool_input[:, where].astype(jnp.float32)], axis=0
+        )
+        running = source
+        for step in range(steps):
+            running = running + jnp.where(same[step], pltpu.roll(running, 2**step, 0), 0.0)
+        pooled = running / count - source
+        mapped[:, where] = pooled[reach:].astype(jnp.bfloat16)
+
+    @pl.loop(0, tp_count)
+    def _(block):
+        where = pl.ds(pl.multiple_of(block * rows, rows), rows)
+        result = jnp.dot(mapped[where, :], pool_map[0], preferred_element_type=jnp.float32)
+        mapped[where, :] = (result * pool_scale[...]).astype(jnp.bfloat16)
+
+    def owner_rows(position):
+        return pl.ds(pl.multiple_of(position * rows, rows), rows)
+
+    mixed_copies = []
+    for peer in (to_x, to_cross, to_core):
+        mixed_copies.append(send(mapped.at[owner_rows(peer["tp"])], mixed_in.at[tp], peer))
+    mixed_in[tp] = mapped[owner_rows(tp), :]
+    load_projection.wait()
+    for copy in mixed_copies:
+        copy.wait_recv()
+
+    @pl.loop(0, 4)
+    def _(step):
+        wide = width // 4
+        block = pl.ds(pl.multiple_of(step * wide, wide), wide)
+        total = skip_scale * residual[:, block].astype(jnp.float32)
+        for group in range(tp_count):
+            total = total + jnp.dot(
+                mixed_in[group],
+                projection[group * pool_width : (group + 1) * pool_width, block],
+                preferred_element_type=jnp.float32,
+            )
+        values_in[:, block] = total
+
+    @pl.loop(0, rows // 64)
+    def _(step):
+        block = pl.ds(pl.multiple_of(step * 64, 64), 64)
+        normed[block, :] = layer_norm(values_in[block, :], mix_gain[...], mix_shift[...]).astype(
+            jnp.bfloat16
+        )
+
+    rows_y1 = send(normed.at[first], rows_in.at[0, first], to_y)
+    rows_z2 = send(normed.at[second], rows_in.at[1, second], to_z)
+    rows_y2 = send(normed.at[second], rows_in.at[0, second], to_y)
+    rows_z1 = send(normed.at[first], rows_in.at[1, first], to_z)
+
+    logits = lax.dot_general(
+        routers[...], normed[...], (((1,), (1,)), ((), ())), preferred_element_type=jnp.float32
+    )
+    group_exp = jnp.exp(logits[expert_count : expert_count + group_count])
+    group_prob = group_exp / jnp.sum(group_exp, axis=0, keepdims=True)
+    group_of = lax.broadcasted_iota(jnp.int32, (expert_count, rows), 0) // (
+        expert_count // group_count
+    )
+    group_share = jnp.zeros((expert_count, rows), jnp.float32)
+    for group in range(group_count):
+        group_share = jnp.where(group_of == group, group_prob[group : group + 1], group_share)
+    picked_exp = jnp.where(named, jnp.exp(jnp.where(named, logits[:expert_count], 0.0)), 0.0)
+    pair_share = picked_exp / jnp.sum(picked_exp, axis=0, keepdims=True)
+    meta[expert_count:, :] = group_share * pair_share
     meta_y = send(meta, meta_in.at[0], to_y)
     meta_z = send(meta, meta_in.at[1], to_z)
-    rows_y1 = send(normed.at[first], rows_in.at[0, first], to_y)
-    rows_z2 = send(normed.at[second], rows_in.at[1, second], to_z)
-    down_far = send(own_down.at[0, mine], down_b.at[mine], to_far)
-    gate_x = send(gate_piece, gate_b.at[:, mine], to_x)
-    up_x = send(up_piece, up_b.at[:, mine], to_x)
-    gate_c = send(gate_piece, gate_b.at[:, mine], to_core)
-    up_c = send(up_piece, up_b.at[:, mine], to_core)
-    keep = [
-        pltpu.make_async_copy(gate_piece, gate_b.at[:, mine], load_sems.at[3]),
-        pltpu.make_async_copy(up_piece, up_b.at[:, mine], load_sems.at[4]),
-    ]
-    for load in keep:
-        load.start()
-    rows_y2 = send(normed.at[second], rows_in.at[0, second], to_y)
-    rows_z1 = send(normed.at[first], rows_in.at[1, first], to_z)
 
     slot_ids = lax.broadcasted_iota(jnp.int32, (slots, rows), 0).astype(jnp.float32)
     experts = (sp, flip(sp, group_size))
@@ -250,24 +355,24 @@
             ).astype(jnp.bfloat16)
 
     own, from_y, from_z, from_corner = 3, 0, 1, 2
+    gate_far.wait_recv()
+    gate_x = send(gate_b.at[:, mine], gate_b.at[:, mine], to_x)
+    gate_c = send(gate_b.at[:, mine], gate_b.at[:, mine], to_core)
     select(own, normed, meta)
     for load in loads:
         load.wait()
     ffn(own, 0, gate_a, up_a, down_a)
 
+    rows_y1.wait_recv()
+    rows_corner1 = send(rows_in.at[0, first], rows_in.at[2, first], to_z)
     meta_y.wait_recv()
     meta_corner = send(meta_in.at[0], meta_in.at[2], to_z)
-    rows_y1.wait_recv()
-    rows_corner1 = send(rows_in.at[0, first], rows_in.at[2, first], to_z)
+    up_far = send(own_up.at[0, :, mine], up_b.at[:, mine], to_far)
+    down_far = send(own_down.at[0, mine], down_b.at[mine], to_far)
     rows_z2.wait_recv()
     rows_corner2 = send(rows_in.at[1, second], rows_in.at[2, second], to_y)
     gate_x.wait_recv()
     gate_relay = send(gate_b.at[:, across], gate_b.at[:, across], to_core)
-    up_x.wait_recv()
-    up_relay = send(up_b.at[:, across], up_b.at[:, across], to_core)
-    down_far.wait_recv()
-    down_x = send(down_b.at[mine], down_b.at[mine], to_x)
-    down_c = send(down_b.at[mine], down_b.at[mine], to_core)
 
     rows_y2.wait_recv()
     select(from_y, rows_in.at[0], meta_in.at[0])
@@ -276,15 +381,21 @@
     rows_z1.wait_recv()
     select(from_z, rows_in.at[1], meta_in.at[1])
     ffn(from_z, 0, gate_a, up_a, down_a)
-    down_x.wait_recv()
-    down_relay = send(down_b.at[across], down_b.at[across], to_core)
+    up_far.wait_recv()
+    up_x = send(up_b.at[:, mine], up_b.at[:, mine], to_x)
+    up_c = send(up_b.at[:, mine], up_b.at[:, mine], to_core)
     meta_corner.wait_recv()
     rows_corner1.wait_recv()
     rows_corner2.wait_recv()
     select(from_corner, rows_in.at[2], meta_in.at[2])
     ffn(from_corner, 0, gate_a, up_a, down_a)
-    for load in keep:
-        load.wait()
+    down_far.wait_recv()
+    down_x = send(down_b.at[mine], down_b.at[mine], to_x)
+    down_c = send(down_b.at[mine], down_b.at[mine], to_core)
+    up_x.wait_recv()
+    up_relay = send(up_b.at[:, across], up_b.at[:, across], to_core)
+    down_x.wait_recv()
+    down_relay = send(down_b.at[across], down_b.at[across], to_core)
     for copy in (gate_c, up_c, gate_relay, up_relay, down_c, down_relay):
         copy.wait_recv()
 
@@ -327,44 +438,53 @@
         copy.wait_send()
 
 
-def routing_table(chosen, weight, expert_count, capacity):
-    rows = chosen.shape[0]
-    half = rows // 2
-    onehot = (
-        chosen[:, :, None] == jnp.arange(expert_count, dtype=jnp.int32)[None, None, :]
-    ).astype(jnp.float32)
-    named = jnp.sum(onehot, axis=1)
-    before = jnp.tril(jnp.ones((half, half), jnp.bfloat16), -1)
-    rank = jnp.einsum(
-        "ab,hbe->hae",
-        before,
-        named.reshape(2, half, expert_count).astype(jnp.bfloat16),
-        preferred_element_type=jnp.float32,
-    )
-    rank = rank + jnp.arange(2, dtype=jnp.float32)[:, None, None] * capacity
-    slot = jnp.where(named > 0, rank.reshape(rows, expert_count), -1.0)
-    share = jnp.sum(onehot * weight[:, :, None], axis=1)
-    return jnp.concatenate([slot, share], axis=1).T
-
-
-def near_experts(
-    normed, weight, routes, pieces, expert_gate, expert_up, expert_down, ffn_gain, ffn_shift
+def whole_layer(
+    residual,
+    pool_input,
+    doc_ids,
+    pool_map,
+    pool_scale,
+    out_weight,
+    mix_gain,
+    mix_shift,
+    group_router,
+    expert_router,
+    expert_gate,
+    expert_up,
+    expert_down,
+    routes,
+    ffn_gain,
+    ffn_shift,
 ):
-    expert_count = lax.axis_size("sp")
-    rows, width = normed.shape
+    expert_count, tp_count = lax.axis_size("sp"), lax.axis_size("tp")
+    rows, width = residual.shape
     ff = expert_gate.shape[2]
-    capacity = rows // 2 * routes.shape[1] * 2 // expert_count
-    slots = 2 * capacity
-    meta = routing_table(routes, weight, expert_count, capacity)
+    seq_rows, pool_width = pool_input.shape
+    group_count = group_router.shape[1]
+    slots = 2 * rows * routes.shape[1] // expert_count
+    reach = 16
+    lanes = 128
+    docs = jnp.broadcast_to(doc_ids[:, None], (seq_rows, lanes))
+    routers = jnp.concatenate([expert_router.T, group_router.T], axis=0)
+    routers = jnp.pad(routers, ((0, 2 * expert_count - routers.shape[0]), (0, 0)))
     vmem = pl.BlockSpec(memory_space=pltpu.VMEM)
     anywhere = pl.BlockSpec(memory_space=pl.ANY)
-    bf16 = jnp.bfloat16
+    bf16, f32 = jnp.bfloat16, jnp.float32
+    table = (2 * expert_count, rows)
     return pl.pallas_call(
-        functools.partial(experts_kernel, (slots, expert_count)),
+        functools.partial(experts_kernel, (slots, expert_count, group_count, tp_count)),
         out_shape=jax.ShapeDtypeStruct((rows, width), bf16),
-        in_specs=[vmem, vmem] + [anywhere] * 5 + [vmem, vmem],
+        in_specs=[vmem] * 5 + [anywhere] + [vmem] * 4 + [anywhere] * 3 + [vmem] * 2,
         out_specs=vmem,
         scratch_shapes=[
+            pltpu.VMEM((reach, pool_width), bf16),
+            pltpu.VMEM((reach, lanes), jnp.int32),
+            pltpu.VMEM((seq_rows, pool_width), bf16),
+            pltpu.VMEM((tp_count, rows, pool_width), bf16),
+            pltpu.VMEM(out_weight.shape, bf16),
+            pltpu.VMEM((rows, width), f32),
+            pltpu.VMEM((rows, width), bf16),
+            pltpu.VMEM(table, f32),
             pltpu.VMEM((width, ff), bf16),
             pltpu.VMEM((width, ff), bf16),
             pltpu.VMEM((ff, width), bf16),
@@ -372,27 +492,33 @@
             pltpu.VMEM((width, ff), bf16),
             pltpu.VMEM((ff, width), bf16),
             pltpu.VMEM((3, rows, width), bf16),
-            pltpu.VMEM((3,) + meta.shape, jnp.float32),
+            pltpu.VMEM((3,) + table, f32),
             pltpu.VMEM((4, 2 * slots, width), bf16),
             pltpu.VMEM((4, rows, 2 * slots), bf16),
-            pltpu.VMEM((4, 2 * slots, 1), jnp.float32),
+            pltpu.VMEM((4, 2 * slots, 1), f32),
             pltpu.VMEM((slots, ff), bf16),
             pltpu.VMEM((4, 2 * slots, width), bf16),
             pltpu.VMEM((3, rows, width), bf16),
             pltpu.VMEM((2, rows // 2, width), bf16),
             pltpu.VMEM((2, rows, width), bf16),
-            pltpu.SemaphoreType.DMA((5,)),
-            pltpu.SemaphoreType.DMA((25,)),
-            pltpu.SemaphoreType.DMA((25,)),
+            pltpu.SemaphoreType.DMA((4,)),
+            pltpu.SemaphoreType.DMA((32,)),
+            pltpu.SemaphoreType.DMA((32,)),
         ],
         compiler_params=pltpu.CompilerParams(
-            collective_id=0, has_side_effects=True, vmem_limit_bytes=60 * 1024 * 1024
+            collective_id=0, has_side_effects=True, vmem_limit_bytes=62 * 1024 * 1024
         ),
     )(
-        normed,
-        meta,
-        pieces[0],
-        pieces[1],
+        residual,
+        pool_input,
+        docs,
+        pool_map,
+        pool_scale[None, :],
+        out_weight,
+        mix_gain[None, :],
+        mix_shift[None, :],
+        routers,
+        routes.T,
         expert_gate,
         expert_up,
         expert_down,
@@ -423,15 +549,25 @@
     reach_rows = 15
     expert_count = lax.axis_size("sp")
     tp_count = lax.axis_size("tp")
-    near = expert_count == 2 * group_size and tp_count == group_size
-    if near:
-        piece = expert_gate.shape[2] // tp_count
-        begin = lax.axis_index("tp") * piece
-        swap = [(i, (i + group_size) % expert_count) for i in range(expert_count)]
-        pieces = [
-            lax.ppermute(lax.dynamic_slice_in_dim(part[0], begin, piece, axis=1), "sp", swap)
-            for part in (expert_gate, expert_up)
-        ]
+    if expert_count == 2 * group_size and tp_count == group_size:
+        return whole_layer(
+            residual,
+            pool_input,
+            doc_ids,
+            pool_map,
+            pool_scale,
+            out_weight,
+            mix_gain,
+            mix_shift,
+            group_router,
+            expert_router,
+            expert_gate,
+            expert_up,
+            expert_down,
+            routes,
+            ffn_gain,
+            ffn_shift,
+        )
     window = jnp.left_shift(jnp.int32(2), lax.axis_index("tp"))
     first_row = lax.axis_index("sp") * seq_rows
     tail_values, tail_docs = from_behind(
@@ -469,10 +605,6 @@
         skip_scale * residual.astype(jnp.float32) + branch, mix_gain, mix_shift
     ).astype(jnp.bfloat16)
     weight = route_weights(normed, routes, group_router, expert_router)
-    if near:
-        return near_experts(
-            normed, weight, routes, pieces, expert_gate, expert_up, expert_down, ffn_gain, ffn_shift
-        )
     half_most = row_count * routes.shape[1] // expert_count
     half_rows = row_count // 2
     routed_parts = []

time: 156 us -> 165 us (1.058)
  Pallas kernels: 93.1 us -> 159 us
  waiting for transfers between devices: 27.1 us -> 0 us
  starting transfers between devices: 14.8 us -> 0 us
  matrix products: 8.99 us -> 0 us
  local copies, waits for them, and re-layouts: 8.95 us -> 3.98 us
    pallas_call x1, Pallas kernels: 93.1 us -> 159 us  [whole_layer(): pl.pallas_call(functools.partial(experts_kernel, (slots, expert_count, gr...]
    ppermute x4 -> x0, waiting for transfers between devices: 18.3 us -> none  [the longest x2 18.3 us: on_device(): lax.ppermute(lax.dynamic_slice_in_dim(part[0], begin, piece, axis=1), 'sp...]
    ppermute x4 -> x0, starting transfers between devices: 11.3 us -> none  [the longest x2 8.31 us: from_behind(): return lax.ppermute(block, axis, route)]
    dot_general x5 -> x0, matrix products: 8.99 us -> none  [the longest x1 4.46 us: on_device(): jnp.dot(pooled, pool_map[0], preferred_element_type=jnp.float32)]
    all_to_all x1 -> x0, waiting for transfers between devices: 8.73 us -> none  [on_device(): lax.all_to_all(blocks, 'tp', split_axis=0, concat_axis=2, tiled=True)]
    all_to_all x1 -> x0, starting transfers between devices: 3.47 us -> none  [on_device(): lax.all_to_all(blocks, 'tp', split_axis=0, concat_axis=2, tiled=True)]
    dynamic_slice x2 -> x0, local copies, waits for them, and re-layouts: 2.94 us -> none  [on_device(): lax.dynamic_slice_in_dim(part[0], begin, piece, axis=1)]
    broadcast_in_dim x0 -> x1, local copies, waits for them, and re-layouts: none -> 1.68 us  [whole_layer(): docs = jnp.broadcast_to(doc_ids[:, None], (seq_rows, lanes))]
  transfers between devices with their start and end apart: 5 -> 0, of which waited for: 3 -> 0; matrix products, arithmetic and copies ran while one was open for 10% -> 0% of each run, Pallas kernels for 0% -> 0%
where the time goes in v2:
time: 165 us
  Pallas kernels  159 us (96%)
  local copies, waits for them, and re-layouts  3.98 us (2%)
    pallas_call x1, Pallas kernels, whole_layer(): pl.pallas_call(functools.partial(experts_kernel, (slots, expert_count, gr...  159 us

profile of v2, /device:TPU:0, one launch (start us, length us, event | category | flops | bytes accessed | tf_op | source)
XLA Modules:
  0.0 164.9 jit_solution(3806081569489407929)
XLA Ops:
  0.0 1.4 fusion.2.routers
  1.4 1.7 %broadcast_in_dim.21.docs = s32[1024,128]{1,0:T(8,128)} broadcast(s32[1024]{0:T(1024)} %param.18), dimensions={0} | broadcast | bytes 528384 | tf_op jit(solution)/shard_map/broadcast_in_dim | solution.py:467
  3.1 159.5 %shard_map.154 = bf16[256,2048]{1,0:T(8,128)(2,1)} custom-call(bf16[256,2048]{1,0:T(8,128)(2,1)} %residual.1, bf16[1024,256]{1,0:T(8,128)(2,1)} %pool_input.1, s32[1024,128]{1,0:T(8,128)} %broadcast_in_dim.21.docs, bf16[1,256,256]{2,1,0:T(8,128)(2,1)} %pool_map.1, f32[1,256]{1,0:T(1,128)} %bitcast.15, bf16[1024,2048]{1,0:T(8,128)(2,1)} %out_weight.1, ...), custom_call_target="tpu_custom_call" | custom-call | tf_op jit(solution)/shard_map/pallas_call | solution.py:474
  162.6 2.3 %copy.18 = bf16[256,2048]{1,0:T(8,128)(2,1)} copy(bf16[256,2048]{1,0:T(8,128)(2,1)} %shard_map.154) | data formatting | bytes 2097152

commit v3 on v2

--- a/solution.py
+++ b/solution.py
@@ -193,12 +193,18 @@
     def cols(position):
         return pl.ds(pl.multiple_of(position * piece, piece), piece)
 
+    def deep(position):
+        size = width // tp_count
+        return pl.ds(pl.multiple_of(position * size, size), size)
+
     mine, across = cols(tp), cols(flip(tp, 2))
+    deep_mine, deep_across = deep(tp), deep(flip(tp, 2))
 
     last = pl.ds(seq_rows - reach, reach)
     tail_copy = send(pool_input.at[last], tail, to_next)
     docs_copy = send(docs.at[last], tail_docs, to_next)
-    gate_far = send(own_gate.at[0, :, mine], gate_b.at[:, mine], to_far)
+    gate_far = send(own_gate.at[0, deep_mine], gate_b.at[deep_mine], to_far)
+    up_far = send(own_up.at[0, deep_mine], up_b.at[deep_mine], to_far)
 
     expert_rows = lax.broadcasted_iota(jnp.int32, (2 * expert_count, rows), 0)
     named = (expert_rows == chosen[0:1, :]) | (expert_rows == chosen[1:2, :])
@@ -296,6 +302,7 @@
     meta[expert_count:, :] = group_share * pair_share
     meta_y = send(meta, meta_in.at[0], to_y)
     meta_z = send(meta, meta_in.at[1], to_z)
+    down_far = send(own_down.at[0, mine], down_b.at[mine], to_far)
 
     slot_ids = lax.broadcasted_iota(jnp.int32, (slots, rows), 0).astype(jnp.float32)
     experts = (sp, flip(sp, group_size))
@@ -356,34 +363,32 @@
 
     own, from_y, from_z, from_corner = 3, 0, 1, 2
     gate_far.wait_recv()
-    gate_x = send(gate_b.at[:, mine], gate_b.at[:, mine], to_x)
-    gate_c = send(gate_b.at[:, mine], gate_b.at[:, mine], to_core)
+    gate_x = send(gate_b.at[deep_mine], gate_b.at[deep_mine], to_x)
+    gate_c = send(gate_b.at[deep_mine], gate_b.at[deep_mine], to_core)
     select(own, normed, meta)
     for load in loads:
         load.wait()
     ffn(own, 0, gate_a, up_a, down_a)
 
     rows_y1.wait_recv()
-    rows_corner1 = send(rows_in.at[0, first], rows_in.at[2, first], to_z)
     meta_y.wait_recv()
-    meta_corner = send(meta_in.at[0], meta_in.at[2], to_z)
-    up_far = send(own_up.at[0, :, mine], up_b.at[:, mine], to_far)
-    down_far = send(own_down.at[0, mine], down_b.at[mine], to_far)
     rows_z2.wait_recv()
     rows_corner2 = send(rows_in.at[1, second], rows_in.at[2, second], to_y)
     gate_x.wait_recv()
-    gate_relay = send(gate_b.at[:, across], gate_b.at[:, across], to_core)
+    gate_relay = send(gate_b.at[deep_across], gate_b.at[deep_across], to_core)
 
     rows_y2.wait_recv()
     select(from_y, rows_in.at[0], meta_in.at[0])
     ffn(from_y, 0, gate_a, up_a, down_a)
     meta_z.wait_recv()
+    meta_corner = send(meta_in.at[1], meta_in.at[2], to_y)
     rows_z1.wait_recv()
+    rows_corner1 = send(rows_in.at[1, first], rows_in.at[2, first], to_y)
     select(from_z, rows_in.at[1], meta_in.at[1])
     ffn(from_z, 0, gate_a, up_a, down_a)
     up_far.wait_recv()
-    up_x = send(up_b.at[:, mine], up_b.at[:, mine], to_x)
-    up_c = send(up_b.at[:, mine], up_b.at[:, mine], to_core)
+    up_x = send(up_b.at[deep_mine], up_b.at[deep_mine], to_x)
+    up_c = send(up_b.at[deep_mine], up_b.at[deep_mine], to_core)
     meta_corner.wait_recv()
     rows_corner1.wait_recv()
     rows_corner2.wait_recv()
@@ -393,7 +398,7 @@
     down_x = send(down_b.at[mine], down_b.at[mine], to_x)
     down_c = send(down_b.at[mine], down_b.at[mine], to_core)
     up_x.wait_recv()
-    up_relay = send(up_b.at[:, across], up_b.at[:, across], to_core)
+    up_relay = send(up_b.at[deep_across], up_b.at[deep_across], to_core)
     down_x.wait_recv()
     down_relay = send(down_b.at[across], down_b.at[across], to_core)
     for copy in (gate_c, up_c, gate_relay, up_relay, down_c, down_relay):

time: 165 us -> 163 us (0.988)
  the two profiles are of different devices: /device:TPU:0 before, /device:TPU:21 now
where the time goes in v3:
time: 163 us
  Pallas kernels  157 us (96%)
  local copies, waits for them, and re-layouts  3.98 us (2%)
    pallas_call x1, Pallas kernels, whole_layer(): pl.pallas_call(functools.partial(experts_kernel, (slots, expert_count, gr...  157 us

profile of v3, /device:TPU:21, one launch (start us, length us, event | category | flops | bytes accessed | tf_op | source)
XLA Modules:
  0.0 162.7 jit_solution(5916575830584308288)
XLA Ops:
  0.0 1.4 fusion.2.routers
  1.4 1.7 %broadcast_in_dim.21.docs = s32[1024,128]{1,0:T(8,128)} broadcast(s32[1024]{0:T(1024)} %param.18), dimensions={0} | broadcast | bytes 528384 | tf_op jit(solution)/shard_map/broadcast_in_dim | solution.py:472
  3.1 157.3 %shard_map.154 = bf16[256,2048]{1,0:T(8,128)(2,1)} custom-call(bf16[256,2048]{1,0:T(8,128)(2,1)} %residual.1, bf16[1024,256]{1,0:T(8,128)(2,1)} %pool_input.1, s32[1024,128]{1,0:T(8,128)} %broadcast_in_dim.21.docs, bf16[1,256,256]{2,1,0:T(8,128)(2,1)} %pool_map.1, f32[1,256]{1,0:T(1,128)} %bitcast.15, bf16[1024,2048]{1,0:T(8,128)(2,1)} %out_weight.1, ...), custom_call_target="tpu_custom_call" | custom-call | tf_op jit(solution)/shard_map/pallas_call | solution.py:479
  160.4 2.3 %copy.18 = bf16[256,2048]{1,0:T(8,128)(2,1)} copy(bf16[256,2048]{1,0:T(8,128)(2,1)} %shard_map.154) | data formatting | bytes 2097152
